TPU v7x, 256 devices: a whole 4x4x8 slice. The times are simulated.
256 devices in a mesh: gr: 2 (over z_hi), sp: 16 (over z_lo, y), tp: 8 (over x, core).
Axes of the slice: x: 4, y: 4, z: 8 (z_hi: 2, z_lo: 4; z = z_hi * 4 + z_lo), core: 2. Of those that a mesh axis runs over, the one named last changes fastest.
Arguments:
- tokens: bfloat16 [8, 3072, 4096], P('gr', 'sp', 'tp'), may hold values from -6.5 to 6.5
- first_token_input: bfloat16 [8, 4096], P('gr', 'sp'), may hold values from -6 to 6
- forget_weight: bfloat16 [4096, 4096], P(None, 'tp'), may hold values from -0.1171875 to 0.1171875
- value_weight: bfloat16 [4096, 4096], P(None, 'tp'), may hold values from -0.375 to 0.375
- query_weight: bfloat16 [4096, 4096], P('sp', 'tp'), may hold values from -0.09375 to 0.09375
- output_gate_weight: bfloat16 [4096, 4096], P('sp', 'tp'), may hold values from -0.09375 to 0.09375
- forget_bound_slack: float32 [4096], P('tp'), may hold values from 0.00016276042 to 0.8, as said below
- additional_damping_exponent: float32 [8, 3072, 32], P('gr', 'sp', 'tp'), may hold values from -2.2 to 0, as said below
- read_norm_scale: float32 [128], replicated, may hold values from 0.1 to 1.9
Outputs:
- cache: bfloat16 [8, 32, 128, 128], P('gr', 'tp', 'sp')
- first_read: bfloat16 [8, 4096], P('gr', 'tp')
Inputs may be any that keep to these rules, and one draw needn't show every extreme that they name: `forget_bound_slack`: positive gaps, one per channel. `additional_damping_exponent`: non-positive log-decays.
All inputs are finite; a program needn't handle non-finite values.
Results may differ from a plain program's by a relative error of at most 0.018.
Values may be sent and summed in bfloat16 or wider, within the bound.
No kernel may reach another device: no remote copies, remote signals or barrier semaphores. Data moves between devices by JAX's collectives and lax.ppermute only.
A program may use at most 64 MiB of HBM per device.

v0:
```python
import jax
import jax.numpy as jnp
from jax import lax
from jax.sharding import PartitionSpec as P


def from_everyone(shard, axis):
    count = lax.axis_size(axis)
    return lax.all_to_all(
        jnp.broadcast_to(shard[None], (count, *shard.shape)), axis, 0, 0, tiled=True
    )


def folded_in_pairs(pieces, combine):
    while len(jax.tree.leaves(pieces)[0]) > 1:
        pieces = jax.vmap(combine)(*(pieces[side::2] for side in (0, 1)))
    return pieces[0]


def prefix(shard, axis, combine, identity):
    count, position = (lax.axis_size(axis), lax.axis_index(axis))
    passed = jnp.arange(count) > position

    def kept(part, zero, own):
        part = jnp.where(
            passed.reshape(-1, *(1 for _ in own.shape)), part, jnp.asarray(zero, own.dtype)
        )
        return part[::-1]

    pieces = from_everyone(shard, axis)
    return folded_in_pairs(kept(pieces, identity, shard), combine)


def cut_along(shard, dim, count):
    shape = shard.shape
    blocks = shard.reshape(*shape[:dim], count, shape[dim] // count, *shape[dim + 1 :])
    return jnp.moveaxis(blocks, dim, 0)


def sent_and_summed(shard, axis, dim):
    count = lax.axis_size(axis)
    blocks = lax.all_to_all(cut_along(shard, dim, count), axis, 0, 0, tiled=True)
    return jnp.sum(blocks.astype(jnp.float32), axis=0)


def of_everyone(shard, axis):
    everything = from_everyone(shard, axis)
    return jnp.sum(everything, axis=0)


def packed_total(arrays, axis):
    ends = [0]
    for a in arrays:
        ends.append(ends[-1] + a.size)
    total = of_everyone(jnp.concatenate([a.ravel() for a in arrays]), axis)
    return tuple((total[b:e].reshape(a.shape) for a, b, e in zip(arrays, ends, ends[1:])))


def add_sums(earlier, later_part):
    return earlier + later_part


def per_device(
    tokens,
    first_token_input,
    forget_weight,
    value_weight,
    query_weight,
    output_gate_weight,
    forget_bound_slack,
    additional_damping_exponent,
    read_norm_scale,
):
    seq_count, block_len, width_part = tokens.shape
    head_dim = read_norm_scale.shape[0]
    local_heads = additional_damping_exponent.shape[2]
    channels = local_heads * head_dim
    flat_rows = tokens.reshape(seq_count * block_len, width_part)
    segment = lax.all_gather(flat_rows, "tp", axis=1, tiled=True)
    forget_acc = jnp.dot(segment, forget_weight, preferred_element_type=jnp.float32)
    value_acc = jnp.dot(segment, value_weight, preferred_element_type=jnp.float32)
    forget = forget_acc.astype(jnp.bfloat16).reshape(seq_count, block_len, channels)
    values = value_acc.astype(jnp.bfloat16).reshape(seq_count, block_len, local_heads, head_dim)
    sp_count = lax.axis_size("sp")
    rows_here = head_dim // sp_count
    row_start = lax.axis_index("sp") * rows_here
    valve_sampler_seeds = forget_bound_slack * jax.nn.sigmoid(-forget.astype(jnp.float32))
    damping_exponent = jnp.log1p(-valve_sampler_seeds) + jnp.repeat(
        additional_damping_exponent, head_dim, axis=2
    )
    totals = jnp.sum(damping_exponent, axis=1)
    later_sum = prefix(totals, "sp", add_sums, jnp.zeros_like(totals))
    within = totals[:, None, :] - jnp.cumsum(damping_exponent, axis=1)
    weighted = (valve_sampler_seeds * jnp.exp(within + later_sum[:, None, :])).astype(jnp.bfloat16)
    weighted = weighted.reshape(seq_count, block_len, local_heads, head_dim)
    state_terms = jnp.einsum(
        "slha,slhb->shab", weighted, values, preferred_element_type=jnp.float32
    )
    state_sum = sent_and_summed(state_terms.astype(jnp.bfloat16), "sp", 2)
    cache_rows = state_sum.astype(jnp.bfloat16)
    slab_rows = first_token_input.shape[1]
    row_first = lax.axis_index("sp") * slab_rows
    forget_rows = lax.dynamic_slice_in_dim(forget_weight, row_first, slab_rows, 0)
    value_rows = lax.dynamic_slice_in_dim(value_weight, row_first, slab_rows, 0)
    new_sums = packed_total(
        (
            jnp.dot(first_token_input, query_weight, preferred_element_type=jnp.float32),
            jnp.dot(first_token_input, output_gate_weight, preferred_element_type=jnp.float32),
            jnp.dot(first_token_input, forget_rows, preferred_element_type=jnp.float32),
            jnp.dot(first_token_input, value_rows, preferred_element_type=jnp.float32),
        ),
        "sp",
    )
    new_query, new_gate, new_forget, new_value = [
        summed.astype(jnp.bfloat16) for summed in new_sums
    ]
    new_keys = (forget_bound_slack * jax.nn.sigmoid(-new_forget.astype(jnp.float32))).reshape(
        seq_count, local_heads, head_dim
    )
    own_keys = lax.dynamic_slice_in_dim(new_keys, row_start, rows_here, 2)
    own_query = lax.dynamic_slice_in_dim(
        new_query.astype(jnp.float32).reshape(seq_count, local_heads, head_dim),
        row_start,
        rows_here,
        2,
    )
    value_new = new_value.astype(jnp.float32).reshape(seq_count, local_heads, head_dim)
    updated = (1.0 - own_keys)[..., None] * cache_rows.astype(jnp.float32) + own_keys[
        ..., None
    ] * value_new[:, :, None, :]
    read_part = jnp.einsum("sha,shab->shb", own_query, updated, precision=lax.Precision.HIGHEST)
    read_sum = of_everyone(read_part, "sp")
    scaled = (
        read_sum
        * lax.rsqrt(jnp.mean(read_sum * read_sum, axis=-1, keepdims=True) + 1e-06)
        * read_norm_scale
    )
    first_read = (
        scaled.reshape(seq_count, channels) * jax.nn.silu(new_gate.astype(jnp.float32))
    ).astype(jnp.bfloat16)
    return (cache_rows, first_read)


def solution(mesh):
    placed = (
        P("gr", "sp", "tp"),
        P("gr", "sp"),
        P(None, "tp"),
        P(None, "tp"),
        P("sp", "tp"),
        P("sp", "tp"),
        P("tp"),
        P("gr", "sp", "tp"),
        P(),
    )
    return jax.shard_map(
        per_device,
        mesh=mesh,
        in_specs=placed,
        out_specs=(P("gr", "tp", "sp", None), P("gr", "tp")),
        check_vma=False,
    )
```

profile of v0, /device:TPU:2, one launch (start us, length us, event | category | flops | bytes accessed | tf_op | source)
XLA Modules:
  0.0 156.7 jit_solution(15677566617659732985)
XLA Ops:
  8.9 1.1 convolution_bitcast_fusion.2
  10.1 1.1 convolution_bitcast_fusion.1
  11.2 1.1 convolution_bitcast_fusion
  12.5 1.0 broadcast_in_dim.20
  13.5 1.8 %reshape.149 = f32[4,192,512]{2,1,0:T(8,128)} reshape(f32[4,192,4,128]{3,2,1,0:T(4,128)S(1)} %broadcast_in_dim.20) | data formatting | bytes 3145728 | tf_op jit(solution)/shard_map/reshape | solution.py:88
  15.3 40.1 %all-gather.2.cloned.1.call-done = bf16[768,4096]{1,0:T(8,128)(2,1)} async-done(((bf16[768,512]{1,0:T(8,128)(2,1)}), bf16[768,4096]{1,0:T(8,128)(2,1)}) %all-gather.2.cloned.1.call-update) | async-done | bytes 6291472 | tf_op jit(solution)/shard_map/all_gather | solution.py:79
  55.3 7.4 %convolution_convert_fusion = bf16[768,512]{1,0:T(8,128)(2,1)S(1)} fusion(bf16[768,4096]{1,0:T(8,128)(2,1)} %all-gather.2.cloned.1.call-done, bf16[4096,512]{1,0:T(8,128)(2,1)} %param.12), kind=kOutput, calls=%fused_computation.10 | convolution fusion | flops 3221618688 | bytes 11272192 | tf_op jit(solution)/shard_map/dot_general | solution.py:81
  62.7 1.1 reshape.153
  63.9 7.0 %add_divide_fusion = f32[768,512]{1,0:T(8,128)S(1)} fusion(bf16[768,4096]{1,0:T(8,128)(2,1)} %all-gather.2.cloned.1.call-done, bf16[4096,512]{1,0:T(8,128)(2,1)} %param.11), kind=kOutput, calls=%fused_computation.9 | convolution fusion | flops 3222798336 | bytes 12058624 | tf_op jit(solution)/shard_map/dot_general | solution.py:80
  71.5 2.4 %add_reduce_fusion = f32[4,4,128]{2,1,0:T(4,128)S(1)} fusion(f32[4,192,4,128]{3,2,1,0:T(4,128)S(1)} %div.22, f32[4,192,4]{2,1,0:T(8,128)} %copy-done.2, f32[4,128]{1,0:T(4,128)S(1)} %bitcast.77), kind=kLoop, calls=%fused_computation.8 | loop fusion | flops 1570816 | bytes 1595392 | tf_op jit(solution)/shard_map/reduce_sum | solution.py:91
  74.6 7.4 %all-to-all-start = ((f32[16,4,512]{2,1,0:T(4,128)}), f32[16,4,512]{2,1,0:T(4,128)S(1)}, u32[]{:S(2)}, u32[]{:S(2)}) async-start(f32[16,4,512]{2,1,0:T(4,128)} %broadcast_in_dim.22), calls=%async_computation | async-start | bytes 262144 | tf_op jit(solution)/shard_map/all_to_all | solution.py:9
  82.0 2.0 %add_bitcast_fusion = f32[4,512,192]{1,2,0:T(8,128)S(1)} fusion(f32[4,192,512]{2,1,0:T(8,128)} %reshape.149, f32[4,192,512]{2,1,0:T(8,128)S(1)} %bitcast.70, f32[512]{0:T(512)S(1)} %copy-done.5), kind=kLoop, calls=%fused_computation.7 | loop fusion | flops 1179648 | bytes 4720640 | tf_op jit(solution)/shard_map/transpose
  84.3 1.6 %fusion = f32[4,512,2,128]{1,2,3,0:T(2,128)S(1)} fusion(f32[4,512,2,128]{1,3,2,0:T(8,128)S(1)} %bitcast.72), kind=kOutput, calls=%fused_computation | output fusion | flops 66584576 | bytes 4194304 | tf_op jit(solution)/shard_map/reduce-window
  85.9 1.3 copy-done.1
  87.3 2.3 %broadcast_add_fusion = f32[4,512,2,128]{1,2,3,0:T(2,128)S(1)} fusion(f32[4,512,2,128]{1,2,3,0:T(2,128)} %copy-done.1, f32[4,512,2]{1,2,0:T(2,128)S(1)} %slice.107), kind=kLoop, calls=%fused_computation.18 | loop fusion | flops 524288 | bytes 4210688 | tf_op jit(solution)/shard_map/reduce_window_sum
  89.7 1.7 %copy.32 = f32[4,512,2,128]{1,3,2,0:T(8,128)} copy(f32[4,512,2,128]{1,2,3,0:T(2,128)S(1)} %broadcast_add_fusion) | data formatting | bytes 4194304 | tf_op jit(solution)/shard_map/reduce_window_sum
  91.4 1.2 broadcast_in_dim.24
  92.6 7.5 %all-to-all-start.2 = ((f32[16,1,8192]{2,1,0:T(1,128)}), f32[16,1,8192]{2,1,0:T(1,128)S(1)}, u32[]{:S(2)}, u32[]{:S(2)}) async-start(f32[16,1,8192]{2,1,0:T(1,128)} %broadcast_in_dim.24), calls=%async_computation.2 | async-start | bytes 1048576 | tf_op jit(solution)/shard_map/all_to_all | solution.py:9
  100.3 2.1 %fusion.6 = bf16[4,4,16,8,128]{4,3,2,1,0:T(8,128)(2,1)S(1)} fusion(bf16[4,192,4,128]{3,2,1,0:T(4,128)(2,1)S(1)} %copy-done.3, f32[4,256,512]{2,1,0:T(8,128)} %bitcast.73, f32[4,192,512]{2,1,0:T(8,128)S(1)} %bitcast.71, f32[4,512]{1,0:T(4,128)S(1)} %fusion.22, f32[4,512]{1,0:T(4,128)S(1)} %bitcast.76, f32[512]{0:T(512)S(1)} %copy-done.5), kind=kOutput, calls=%fused_computation.13 | convolution fusion | flops 102891520 | bytes 4474880 | tf_op jit(solution)/shard_map/slha,slhb->shab/dot_general | solution.py:96
  103.3 12.0 %all-to-all-done.2 = f32[16,1,8192]{2,1,0:T(1,128)S(1)} async-done(((f32[16,1,8192]{2,1,0:T(1,128)}), f32[16,1,8192]{2,1,0:T(1,128)S(1)}, u32[]{:S(2)}, u32[]{:S(2)}) %all-to-all-start.2) | async-done | bytes 524320 | tf_op jit(solution)/shard_map/all_to_all | solution.py:9
  115.3 4.6 %all-to-all-start.1 = ((bf16[16,4,4,8,128]{4,3,2,1,0:T(8,128)(2,1)}), bf16[16,4,4,8,128]{4,3,2,1,0:T(8,128)(2,1)S(1)}, u32[]{:S(2)}, u32[]{:S(2)}) async-start(bf16[16,4,4,8,128]{4,3,2,1,0:T(8,128)(2,1)} %bitcast.68), calls=%async_computation.1 | async-start | bytes 1048576 | tf_op jit(solution)/shard_map/all_to_all | solution.py:42
  120.6 14.1 %all-to-all-done.1 = bf16[16,4,4,8,128]{4,3,2,1,0:T(8,128)(2,1)S(1)} async-done(((bf16[16,4,4,8,128]{4,3,2,1,0:T(8,128)(2,1)}), bf16[16,4,4,8,128]{4,3,2,1,0:T(8,128)(2,1)S(1)}, u32[]{:S(2)}, u32[]{:S(2)}) %all-to-all-start.1) | async-done | bytes 524320 | tf_op jit(solution)/shard_map/all_to_all | solution.py:42
  135.7 4.4 %all-to-all-start.3 = ((f32[16,4,4,128]{3,2,1,0:T(4,128)}), f32[16,4,4,128]{3,2,1,0:T(4,128)S(1)}, u32[]{:S(2)}, u32[]{:S(2)}) async-start(f32[16,4,4,128]{3,2,1,0:T(4,128)} %broadcast_in_dim.25), calls=%async_computation.3 | async-start | bytes 262144 | tf_op jit(solution)/shard_map/all_to_all | solution.py:9
  140.2 8.9 %all-to-all-done.3 = f32[16,4,4,128]{3,2,1,0:T(4,128)S(1)} async-done(((f32[16,4,4,128]{3,2,1,0:T(4,128)}), f32[16,4,4,128]{3,2,1,0:T(4,128)S(1)}, u32[]{:S(2)}, u32[]{:S(2)}) %all-to-all-start.3) | async-done | bytes 131104 | tf_op jit(solution)/shard_map/all_to_all | solution.py:9
  (61 shorter events, 7.2 us)
Async XLA Ops:
  7.2 1.0 copy-start
  7.2 4.0 %copy-start.4 = (bf16[4,256]{1,0:T(4,128)(2,1)S(1)}, bf16[4,256]{1,0:T(4,128)(2,1)}, u32[]{:S(2)}) copy-start(bf16[4,256]{1,0:T(4,128)(2,1)} %param.10) | copy-start | bytes 6148
  7.2 5.1 %copy-start.7 = (f32[4,192,4]{1,2,0:T(4,128)S(1)}, f32[4,192,4]{1,2,0:T(4,128)}, u32[]{:S(2)}) copy-start(f32[4,192,4]{1,2,0:T(4,128)} %param.16) | copy-start | bytes 36868
  7.2 48.1 %all-gather.2.cloned.1.call-start = ((), (), s32[]{:S(2)}) async-start(), calls=%async_computation.4 | async-start | bytes 7077888 | tf_op jit(solution)/shard_map/all_gather | solution.py:79
  12.5 2.8 %copy-start.2 = (f32[4,192,4]{2,1,0:T(8,128)}, f32[4,192,4]{2,1,0:T(8,128)S(1)}, u32[]{:S(2)}) copy-start(f32[4,192,4]{2,1,0:T(8,128)S(1)} %copy.30) | copy-start | bytes 36868
  70.8 0.7 copy-start.5
  74.6 16.8 %all-to-all-start = ((f32[16,4,512]{2,1,0:T(4,128)}), f32[16,4,512]{2,1,0:T(4,128)S(1)}, u32[]{:S(2)}, u32[]{:S(2)}) async-start(f32[16,4,512]{2,1,0:T(4,128)} %broadcast_in_dim.22), calls=%async_computation | async-start | bytes 262144 | tf_op jit(solution)/shard_map/all_to_all | solution.py:9
  85.9 1.3 copy-start.1
  91.4 8.9 %copy-start.3 = (bf16[4,192,4,128]{3,2,1,0:T(4,128)(2,1)S(1)}, bf16[4,192,4,128]{3,2,1,0:T(4,128)(2,1)}, u32[]{:S(2)}) copy-start(bf16[4,192,4,128]{3,2,1,0:T(4,128)(2,1)} %reshape.153) | copy-start | bytes 2359300
  92.6 22.8 %all-to-all-start.2 = ((f32[16,1,8192]{2,1,0:T(1,128)}), f32[16,1,8192]{2,1,0:T(1,128)S(1)}, u32[]{:S(2)}, u32[]{:S(2)}) async-start(f32[16,1,8192]{2,1,0:T(1,128)} %broadcast_in_dim.24), calls=%async_computation.2 | async-start | bytes 1048576 | tf_op jit(solution)/shard_map/all_to_all | solution.py:9
  115.3 24.8 %copy-start.8 = (f32[128]{0:T(128)S(1)}, f32[128]{0:T(128)}, u32[]{:S(2)}) copy-start(f32[128]{0:T(128)} %param.17) | copy-start | bytes 1540
  115.3 19.3 %all-to-all-start.1 = ((bf16[16,4,4,8,128]{4,3,2,1,0:T(8,128)(2,1)}), bf16[16,4,4,8,128]{4,3,2,1,0:T(8,128)(2,1)S(1)}, u32[]{:S(2)}, u32[]{:S(2)}) async-start(bf16[16,4,4,8,128]{4,3,2,1,0:T(8,128)(2,1)} %bitcast.68), calls=%async_computation.1 | async-start | bytes 1048576 | tf_op jit(solution)/shard_map/all_to_all | solution.py:42
  134.8 15.1 %copy-start.6 = (bf16[4,4,8,128]{3,2,1,0:T(8,128)(2,1)}, bf16[4,4,8,128]{3,2,1,0:T(8,128)(2,1)S(1)}, u32[]{:S(2)}) copy-start(bf16[4,4,8,128]{3,2,1,0:T(8,128)(2,1)S(1)} %reduce_sum.49) | copy-start | bytes 98308
  135.7 13.4 %all-to-all-start.3 = ((f32[16,4,4,128]{3,2,1,0:T(4,128)}), f32[16,4,4,128]{3,2,1,0:T(4,128)S(1)}, u32[]{:S(2)}, u32[]{:S(2)}) async-start(f32[16,4,4,128]{3,2,1,0:T(4,128)} %broadcast_in_dim.25), calls=%async_computation.3 | async-start | bytes 262144 | tf_op jit(solution)/shard_map/all_to_all | solution.py:9
Sparse Core Ops, SparseCore 0:
  9.8 45.4 all-gather.1
where the time goes:
time: 157 us
  waiting for transfers between devices  75.7 us (48%)
  starting transfers between devices  24 us (15%)
  matrix products  20.8 us (13%)
  between operations  14.3 us (9%)
  local copies, waits for them, and re-layouts  11.9 us (8%)
  other arithmetic  10 us (6%)
    all_gather x1, waiting for transfers between devices, per_device(): segment = lax.all_gather(flat_rows, 'tp', axis=1, tiled=True)  40.1 us
    all_to_all x3, waiting for transfers between devices, from_everyone(): lax.all_to_all(jnp.broadcast_to(shard[None], (count, *shard.shape)), axis...  20.9 us
    all_to_all x3, starting transfers between devices, from_everyone(): lax.all_to_all(jnp.broadcast_to(shard[None], (count, *shard.shape)), axis...  19.3 us
    all_to_all x1, waiting for transfers between devices, sent_and_summed(): lax.all_to_all(cut_along(shard, dim, count), axis, 0, 0, tiled=True)  14.1 us
    dot_general x1, matrix products, per_device(): jnp.dot(segment, value_weight, preferred_element_type=jnp.float32)  7.4 us
    dot_general x1, matrix products, per_device(): jnp.dot(segment, forget_weight, preferred_element_type=jnp.float32)  6.97 us
    all_to_all x1, starting transfers between devices, sent_and_summed(): lax.all_to_all(cut_along(shard, dim, count), axis, 0, 0, tiled=True)  4.63 us
    another operation x3, other arithmetic  4.02 us
  transfers between devices with their start and end apart: 5, of which 4 were waited for; matrix products, arithmetic and copies ran while one was open for 12% of the time, Pallas kernels for 0%

commit v1 on v0

--- a/solution.py
+++ b/solution.py
@@ -76,7 +76,14 @@
     local_heads = additional_damping_exponent.shape[2]
     channels = local_heads * head_dim
     flat_rows = tokens.reshape(seq_count * block_len, width_part)
-    segment = lax.all_gather(flat_rows, "tp", axis=1, tiled=True)
+    x = flat_rows
+    ways, here, lap = (lax.axis_size("tp"), lax.axis_index("tp"), x.shape[1])
+    lengths = [n * ways if d == 1 else n for d, n in enumerate(x.shape)]
+    full = lax.dynamic_update_slice_in_dim(jnp.zeros(lengths, x.dtype), x, here * lap, axis=1)
+    for far in range(1, ways):
+        x = lax.ppermute(x, "tp", [(d, (d + 1) % ways) for d in range(ways)])
+        full = lax.dynamic_update_slice_in_dim(full, x, (here - far) % ways * lap, axis=1)
+    segment = full
     forget_acc = jnp.dot(segment, forget_weight, preferred_element_type=jnp.float32)
     value_acc = jnp.dot(segment, value_weight, preferred_element_type=jnp.float32)
     forget = forget_acc.astype(jnp.bfloat16).reshape(seq_count, block_len, channels)

time: 157 us -> 179 us (1.14)
  the two profiles are of different devices: /device:TPU:2 before, /device:TPU:8 now
where the time goes in v1:
time: 179 us; the launch traced here: 178 us
  waiting for transfers between devices  105 us (59%)
  starting transfers between devices  30 us (17%)
  local copies, waits for them, and re-layouts  18.4 us (10%)
  matrix products  12.8 us (7%)
  other arithmetic  10.6 us (6%)
    ppermute x7, waiting for transfers between devices, per_device(): x = lax.ppermute(x, 'tp', [(d, (d + 1) % ways) for d in range(ways)])  77.9 us
    all_to_all x3, starting transfers between devices, from_everyone(): lax.all_to_all(jnp.broadcast_to(shard[None], (count, *shard.shape)), axis...  21.7 us
    all_to_all x3, waiting for transfers between devices, from_everyone(): lax.all_to_all(jnp.broadcast_to(shard[None], (count, *shard.shape)), axis...  15.9 us
    all_to_all x1, waiting for transfers between devices, sent_and_summed(): lax.all_to_all(cut_along(shard, dim, count), axis, 0, 0, tiled=True)  11.3 us
    all_to_all x1, starting transfers between devices, sent_and_summed(): lax.all_to_all(cut_along(shard, dim, count), axis, 0, 0, tiled=True)  8.25 us
    unnamed x38, local copies, waits for them, and re-layouts  4.57 us
    dot_general x1, matrix products, per_device(): jnp.dot(segment, value_weight, preferred_element_type=jnp.float32)  4.35 us
    another operation x3, other arithmetic  4.01 us
  transfers between devices with their start and end apart: 11, of which 10 were waited for; matrix products, arithmetic and copies ran while one was open for 13% of the time, Pallas kernels for 0%

profile of v1, /device:TPU:8, one launch (start us, length us, event | category | flops | bytes accessed | tf_op | source)
XLA Modules:
  0.0 178.0 jit_solution(2939625602254514372)
XLA Ops:
  0.7 12.8 %collective-permute-done = bf16[768,512]{1,0:T(8,128)(2,1)S(1)} collective-permute-done((bf16[768,512]{1,0:T(8,128)(2,1)}, bf16[768,512]{1,0:T(8,128)(2,1)S(1)}, u32[]{:S(2)}, u32[]{:S(2)}) %collective-permute-start) | collective-permute-done | bytes 786464 | tf_op jit(solution)/shard_map/ppermute | solution.py:84
  13.5 12.6 %collective-permute-done.1 = bf16[768,512]{1,0:T(8,128)(2,1)S(1)} collective-permute-done((bf16[768,512]{1,0:T(8,128)(2,1)S(1)}, bf16[768,512]{1,0:T(8,128)(2,1)S(1)}, u32[]{:S(2)}, u32[]{:S(2)}) %collective-permute-start.1) | collective-permute-done | bytes 786464 | tf_op jit(solution)/shard_map/ppermute | solution.py:84
  27.0 12.6 %collective-permute-done.2 = bf16[768,512]{1,0:T(8,128)(2,1)S(1)} collective-permute-done((bf16[768,512]{1,0:T(8,128)(2,1)S(1)}, bf16[768,512]{1,0:T(8,128)(2,1)S(1)}, u32[]{:S(2)}, u32[]{:S(2)}) %collective-permute-start.2) | collective-permute-done | bytes 786464 | tf_op jit(solution)/shard_map/ppermute | solution.py:84
  40.5 12.7 %collective-permute-done.3 = bf16[768,512]{1,0:T(8,128)(2,1)} collective-permute-done((bf16[768,512]{1,0:T(8,128)(2,1)S(1)}, bf16[768,512]{1,0:T(8,128)(2,1)}, u32[]{:S(2)}, u32[]{:S(2)}) %collective-permute-start.3) | collective-permute-done | bytes 786464 | tf_op jit(solution)/shard_map/ppermute | solution.py:84
  55.2 1.8 %reshape.149 = f32[4,192,512]{2,1,0:T(8,128)} reshape(f32[4,192,4,128]{3,2,1,0:T(4,128)S(1)} %broadcast_in_dim.23) | data formatting | bytes 3145728 | tf_op jit(solution)/shard_map/reshape | solution.py:95
  56.9 9.2 %collective-permute-done.4 = bf16[768,512]{1,0:T(8,128)(2,1)} collective-permute-done((bf16[768,512]{1,0:T(8,128)(2,1)}, bf16[768,512]{1,0:T(8,128)(2,1)}, u32[]{:S(2)}, u32[]{:S(2)}) %collective-permute-start.4) | collective-permute-done | bytes 786464 | tf_op jit(solution)/shard_map/ppermute | solution.py:84
  70.6 8.4 %collective-permute-done.5 = bf16[768,512]{1,0:T(8,128)(2,1)S(1)} collective-permute-done((bf16[768,512]{1,0:T(8,128)(2,1)}, bf16[768,512]{1,0:T(8,128)(2,1)S(1)}, u32[]{:S(2)}, u32[]{:S(2)}) %collective-permute-start.5) | collective-permute-done | bytes 786464 | tf_op jit(solution)/shard_map/ppermute | solution.py:84
  82.2 9.5 %collective-permute-done.6 = bf16[768,512]{1,0:T(8,128)(2,1)S(1)} collective-permute-done((bf16[768,512]{1,0:T(8,128)(2,1)S(1)}, bf16[768,512]{1,0:T(8,128)(2,1)S(1)}, u32[]{:S(2)}, u32[]{:S(2)}) %collective-permute-start.6) | collective-permute-done | bytes 786464 | tf_op jit(solution)/shard_map/ppermute | solution.py:84
  91.8 3.6 %add_divide_fusion = f32[768,512]{1,0:T(8,128)S(1)} fusion(bf16[768,4096]{1,0:T(8,128)(2,1)S(1)} %constant_dynamic-update-slice_fusion, bf16[4096,512]{1,0:T(8,128)(2,1)S(1)} %copy-done.13), kind=kOutput, calls=%fused_computation.9 | convolution fusion | flops 3222798336 | bytes 12058624 | tf_op jit(solution)/shard_map/dot_general | solution.py:87
  95.4 4.4 %convolution_convert_fusion = bf16[768,512]{1,0:T(8,128)(2,1)} fusion(bf16[768,4096]{1,0:T(8,128)(2,1)S(1)} %constant_dynamic-update-slice_fusion, bf16[4096,512]{1,0:T(8,128)(2,1)S(1)} %copy-done.14), kind=kOutput, calls=%fused_computation.10 | convolution fusion | flops 3221618688 | bytes 11272192 | tf_op jit(solution)/shard_map/dot_general | solution.py:88
  100.5 2.4 %add_reduce_fusion = f32[4,4,128]{2,1,0:T(4,128)S(1)} fusion(f32[4,192,4,128]{3,2,1,0:T(4,128)S(1)} %div.22, f32[4,192,4]{2,1,0:T(8,128)} %copy-done.2, f32[4,128]{1,0:T(4,128)S(1)} %bitcast.78), kind=kLoop, calls=%fused_computation.8 | loop fusion | flops 1570816 | bytes 1595392 | tf_op jit(solution)/shard_map/reduce_sum | solution.py:98
  103.6 9.0 %all-to-all-start = ((f32[16,4,512]{2,1,0:T(4,128)}), f32[16,4,512]{2,1,0:T(4,128)S(1)}, u32[]{:S(2)}, u32[]{:S(2)}) async-start(f32[16,4,512]{2,1,0:T(4,128)} %broadcast_in_dim.25), calls=%async_computation | async-start | bytes 262144 | tf_op jit(solution)/shard_map/all_to_all | solution.py:9
  112.5 2.0 %add_bitcast_fusion = f32[4,512,192]{1,2,0:T(8,128)S(1)} fusion(f32[4,192,512]{2,1,0:T(8,128)} %reshape.149, f32[4,192,512]{2,1,0:T(8,128)S(1)} %bitcast.70, f32[512]{0:T(512)S(1)} %copy-done.11), kind=kLoop, calls=%fused_computation.7 | loop fusion | flops 1179648 | bytes 4720640 | tf_op jit(solution)/shard_map/transpose
  114.8 1.6 fusion
  117.9 2.3 %broadcast_add_fusion = f32[4,512,2,128]{1,2,3,0:T(2,128)S(1)} fusion(f32[4,512,2,128]{1,2,3,0:T(2,128)} %copy-done.1, f32[4,512,2]{1,2,0:T(2,128)S(1)} %slice.107), kind=kLoop, calls=%fused_computation.18 | loop fusion | flops 524288 | bytes 4210688 | tf_op jit(solution)/shard_map/reduce_window_sum
  120.2 1.7 copy.32
  122.1 2.0 %broadcast_in_dim.27 = f32[16,1,8192]{2,1,0:T(1,128)} broadcast(f32[8192]{0:T(1024)} %pad_maximum_fusion), dimensions={2} | broadcast | bytes 557056 | tf_op jit(solution)/shard_map/broadcast_in_dim | solution.py:10
  124.1 7.5 %all-to-all-start.2 = ((f32[16,1,8192]{2,1,0:T(1,128)}), f32[16,1,8192]{2,1,0:T(1,128)S(1)}, u32[]{:S(2)}, u32[]{:S(2)}) async-start(f32[16,1,8192]{2,1,0:T(1,128)} %broadcast_in_dim.27), calls=%async_computation.2 | async-start | bytes 1048576 | tf_op jit(solution)/shard_map/all_to_all | solution.py:9
  131.8 2.1 %fusion.6 = bf16[4,4,16,8,128]{4,3,2,1,0:T(8,128)(2,1)S(1)} fusion(bf16[4,192,4,128]{3,2,1,0:T(4,128)(2,1)S(1)} %reshape.153, f32[4,256,512]{2,1,0:T(8,128)} %bitcast.73, f32[4,192,512]{2,1,0:T(8,128)S(1)} %bitcast.71, f32[4,512]{1,0:T(4,128)S(1)} %fusion.22, f32[4,512]{1,0:T(4,128)S(1)} %bitcast.77, f32[512]{0:T(512)S(1)} %copy-done.11), kind=kOutput, calls=%fused_computation.13 | convolution fusion | flops 102891520 | bytes 4474880 | tf_op jit(solution)/shard_map/slha,slhb->shab/dot_general | solution.py:103
  134.8 8.4 %all-to-all-done.2 = f32[16,1,8192]{2,1,0:T(1,128)S(1)} async-done(((f32[16,1,8192]{2,1,0:T(1,128)}), f32[16,1,8192]{2,1,0:T(1,128)S(1)}, u32[]{:S(2)}, u32[]{:S(2)}) %all-to-all-start.2) | async-done | bytes 524320 | tf_op jit(solution)/shard_map/all_to_all | solution.py:9
  143.2 8.2 %all-to-all-start.1 = ((bf16[16,4,4,8,128]{4,3,2,1,0:T(8,128)(2,1)}), bf16[16,4,4,8,128]{4,3,2,1,0:T(8,128)(2,1)S(1)}, u32[]{:S(2)}, u32[]{:S(2)}) async-start(bf16[16,4,4,8,128]{4,3,2,1,0:T(8,128)(2,1)} %bitcast.68), calls=%async_computation.1 | async-start | bytes 1048576 | tf_op jit(solution)/shard_map/all_to_all | solution.py:42
  152.1 11.3 %all-to-all-done.1 = bf16[16,4,4,8,128]{4,3,2,1,0:T(8,128)(2,1)S(1)} async-done(((bf16[16,4,4,8,128]{4,3,2,1,0:T(8,128)(2,1)}), bf16[16,4,4,8,128]{4,3,2,1,0:T(8,128)(2,1)S(1)}, u32[]{:S(2)}, u32[]{:S(2)}) %all-to-all-start.1) | async-done | bytes 524320 | tf_op jit(solution)/shard_map/all_to_all | solution.py:42
  164.4 5.2 %all-to-all-start.3 = ((f32[16,4,4,128]{3,2,1,0:T(4,128)}), f32[16,4,4,128]{3,2,1,0:T(4,128)S(1)}, u32[]{:S(2)}, u32[]{:S(2)}) async-start(f32[16,4,4,128]{3,2,1,0:T(4,128)} %broadcast_in_dim.28), calls=%async_computation.3 | async-start | bytes 262144 | tf_op jit(solution)/shard_map/all_to_all | solution.py:9
  169.6 7.5 %all-to-all-done.3 = f32[16,4,4,128]{3,2,1,0:T(4,128)S(1)} async-done(((f32[16,4,4,128]{3,2,1,0:T(4,128)}), f32[16,4,4,128]{3,2,1,0:T(4,128)S(1)}, u32[]{:S(2)}, u32[]{:S(2)}) %all-to-all-start.3) | async-done | bytes 131104 | tf_op jit(solution)/shard_map/all_to_all | solution.py:9
  (95 shorter events, 18.0 us)
Async XLA Ops:
  0.6 67.8 %copy-start = (bf16[256,512]{1,0:T(8,128)(2,1)S(1)}, bf16[256,512]{1,0:T(8,128)(2,1)}, u32[]{:S(2)}) copy-start(bf16[256,512]{1,0:T(8,128)(2,1)} %param.13) | copy-start | bytes 786436
  0.6 12.8 %collective-permute-start = (bf16[768,512]{1,0:T(8,128)(2,1)}, bf16[768,512]{1,0:T(8,128)(2,1)S(1)}, u32[]{:S(2)}, u32[]{:S(2)}) collective-permute-start(bf16[768,512]{1,0:T(8,128)(2,1)} %bitcast.74), channel_id=1, source_target_pairs={{0,1},{1,2},{2,3},{3,4},{4,5},{5,6},{6,7},{7,0},{8,9},{9,10},{10,1... | collective-permute-start | bytes 2359304 | tf_op jit(solution)/shard_map/ppermute | solution.py:84
  13.5 12.6 %collective-permute-start.1 = (bf16[768,512]{1,0:T(8,128)(2,1)S(1)}, bf16[768,512]{1,0:T(8,128)(2,1)S(1)}, u32[]{:S(2)}, u32[]{:S(2)}) collective-permute-start(bf16[768,512]{1,0:T(8,128)(2,1)S(1)} %collective-permute-done), channel_id=1, source_target_pairs={{0,1},{1,2},{2,3},{3,4},{4,5},{5,6},{6,7},{7,0},{8,9},{9,10},{10,1... | collective-permute-start | bytes 2359304 | tf_op jit(solution)/shard_map/ppermute | solution.py:84
  27.0 12.6 %collective-permute-start.2 = (bf16[768,512]{1,0:T(8,128)(2,1)S(1)}, bf16[768,512]{1,0:T(8,128)(2,1)S(1)}, u32[]{:S(2)}, u32[]{:S(2)}) collective-permute-start(bf16[768,512]{1,0:T(8,128)(2,1)S(1)} %collective-permute-done.1), channel_id=1, source_target_pairs={{0,1},{1,2},{2,3},{3,4},{4,5},{5,6},{6,7},{7,0},{8,9},{9,10},{10,1... | collective-permute-start | bytes 2359304 | tf_op jit(solution)/shard_map/ppermute | solution.py:84
  40.5 12.7 %collective-permute-start.3 = (bf16[768,512]{1,0:T(8,128)(2,1)S(1)}, bf16[768,512]{1,0:T(8,128)(2,1)}, u32[]{:S(2)}, u32[]{:S(2)}) collective-permute-start(bf16[768,512]{1,0:T(8,128)(2,1)S(1)} %collective-permute-done.2), channel_id=1, source_target_pairs={{0,1},{1,2},{2,3},{3,4},{4,5},{5,6},{6,7},{7,0},{8,9},{9,10},{10,1... | collective-permute-start | bytes 2359304 | tf_op jit(solution)/shard_map/ppermute | solution.py:84
  53.2 12.9 %collective-permute-start.4 = (bf16[768,512]{1,0:T(8,128)(2,1)}, bf16[768,512]{1,0:T(8,128)(2,1)}, u32[]{:S(2)}, u32[]{:S(2)}) collective-permute-start(bf16[768,512]{1,0:T(8,128)(2,1)} %collective-permute-done.3), channel_id=1, source_target_pairs={{0,1},{1,2},{2,3},{3,4},{4,5},{5,6},{6,7},{7,0},{8,9},{9,10},{10,1... | collective-permute-start | bytes 2359304 | tf_op jit(solution)/shard_map/ppermute | solution.py:84
  54.1 2.8 %copy-start.2 = (f32[4,192,4]{2,1,0:T(8,128)}, f32[4,192,4]{2,1,0:T(8,128)S(1)}, u32[]{:S(2)}) copy-start(f32[4,192,4]{2,1,0:T(8,128)S(1)} %copy.30) | copy-start | bytes 36868
  54.2 12.0 %copy-start.10 = (bf16[4,256]{1,0:T(4,128)(2,1)S(1)}, bf16[4,256]{1,0:T(4,128)(2,1)}, u32[]{:S(2)}) copy-start(bf16[4,256]{1,0:T(4,128)(2,1)} %param.10) | copy-start | bytes 6148
  55.1 13.4 %copy-start.9 = (bf16[256,512]{1,0:T(8,128)(2,1)S(1)}, bf16[256,512]{1,0:T(8,128)(2,1)}, u32[]{:S(2)}) copy-start(bf16[256,512]{1,0:T(8,128)(2,1)} %param.14) | copy-start | bytes 786436
  66.2 12.8 %collective-permute-start.5 = (bf16[768,512]{1,0:T(8,128)(2,1)}, bf16[768,512]{1,0:T(8,128)(2,1)S(1)}, u32[]{:S(2)}, u32[]{:S(2)}) collective-permute-start(bf16[768,512]{1,0:T(8,128)(2,1)} %collective-permute-done.4), channel_id=1, source_target_pairs={{0,1},{1,2},{2,3},{3,4},{4,5},{5,6},{6,7},{7,0},{8,9},{9,10},{10,1... | collective-permute-start | bytes 2359304 | tf_op jit(solution)/shard_map/ppermute | solution.py:84
  69.3 1.1 copy-start.3
  70.5 8.7 %copy-start.5 = (bf16[768,512]{1,0:T(8,128)(2,1)S(1)}, bf16[768,512]{1,0:T(8,128)(2,1)}, u32[]{:S(2)}) copy-start(bf16[768,512]{1,0:T(8,128)(2,1)} %copy-done.4) | copy-start | bytes 2359300
  70.5 8.8 %copy-start.7 = (bf16[768,512]{1,0:T(8,128)(2,1)S(1)}, bf16[768,512]{1,0:T(8,128)(2,1)}, u32[]{:S(2)}) copy-start(bf16[768,512]{1,0:T(8,128)(2,1)} %copy-done.6) | copy-start | bytes 2359300
  79.0 12.6 %collective-permute-start.6 = (bf16[768,512]{1,0:T(8,128)(2,1)S(1)}, bf16[768,512]{1,0:T(8,128)(2,1)S(1)}, u32[]{:S(2)}, u32[]{:S(2)}) collective-permute-start(bf16[768,512]{1,0:T(8,128)(2,1)S(1)} %collective-permute-done.5), channel_id=1, source_target_pairs={{0,1},{1,2},{2,3},{3,4},{4,5},{5,6},{6,7},{7,0},{8,9},{9,10},{10,1... | collective-permute-start | bytes 2359304 | tf_op jit(solution)/shard_map/ppermute | solution.py:84
  80.6 11.1 %copy-start.13 = (bf16[4096,512]{1,0:T(8,128)(2,1)S(1)}, bf16[4096,512]{1,0:T(8,128)(2,1)}, u32[]{:S(2)}) copy-start(bf16[4096,512]{1,0:T(8,128)(2,1)} %param.11) | copy-start | bytes 12582916
  91.8 3.7 %copy-start.14 = (bf16[4096,512]{1,0:T(8,128)(2,1)S(1)}, bf16[4096,512]{1,0:T(8,128)(2,1)}, u32[]{:S(2)}) copy-start(bf16[4096,512]{1,0:T(8,128)(2,1)} %param.12) | copy-start | bytes 12582916
  103.6 18.6 %all-to-all-start = ((f32[16,4,512]{2,1,0:T(4,128)}), f32[16,4,512]{2,1,0:T(4,128)S(1)}, u32[]{:S(2)}, u32[]{:S(2)}) async-start(f32[16,4,512]{2,1,0:T(4,128)} %broadcast_in_dim.25), calls=%async_computation | async-start | bytes 262144 | tf_op jit(solution)/shard_map/all_to_all | solution.py:9
  116.5 1.3 copy-start.1
  120.2 1.7 copy-start.8
  124.1 19.1 %all-to-all-start.2 = ((f32[16,1,8192]{2,1,0:T(1,128)}), f32[16,1,8192]{2,1,0:T(1,128)S(1)}, u32[]{:S(2)}, u32[]{:S(2)}) async-start(f32[16,1,8192]{2,1,0:T(1,128)} %broadcast_in_dim.27), calls=%async_computation.2 | async-start | bytes 1048576 | tf_op jit(solution)/shard_map/all_to_all | solution.py:9
  133.9 35.7 %copy-start.15 = (f32[128]{0:T(128)S(1)}, f32[128]{0:T(128)}, u32[]{:S(2)}) copy-start(f32[128]{0:T(128)} %param.17) | copy-start | bytes 1540
  143.2 20.2 %all-to-all-start.1 = ((bf16[16,4,4,8,128]{4,3,2,1,0:T(8,128)(2,1)}), bf16[16,4,4,8,128]{4,3,2,1,0:T(8,128)(2,1)S(1)}, u32[]{:S(2)}, u32[]{:S(2)}) async-start(bf16[16,4,4,8,128]{4,3,2,1,0:T(8,128)(2,1)} %bitcast.68), calls=%async_computation.1 | async-start | bytes 1048576 | tf_op jit(solution)/shard_map/all_to_all | solution.py:42
  163.5 14.5 %copy-start.12 = (bf16[4,4,8,128]{3,2,1,0:T(8,128)(2,1)}, bf16[4,4,8,128]{3,2,1,0:T(8,128)(2,1)S(1)}, u32[]{:S(2)}) copy-start(bf16[4,4,8,128]{3,2,1,0:T(8,128)(2,1)S(1)} %reduce_sum.49) | copy-start | bytes 98308
  164.4 12.7 %all-to-all-start.3 = ((f32[16,4,4,128]{3,2,1,0:T(4,128)}), f32[16,4,4,128]{3,2,1,0:T(4,128)S(1)}, u32[]{:S(2)}, u32[]{:S(2)}) async-start(f32[16,4,4,128]{3,2,1,0:T(4,128)} %broadcast_in_dim.28), calls=%async_computation.3 | async-start | bytes 262144 | tf_op jit(solution)/shard_map/all_to_all | solution.py:9
  (3 other events, 2.4 us)
